TPU v7x, 512 devices: a whole 4x4x16 slice. The times are simulated.
512 devices in a mesh: sp: 16 (over z), dp: 32 (over y, x, core).
Axes of the slice: x: 4, y: 4, z: 16, core: 2. Of those that a mesh axis runs over, the one named last changes fastest.
Arguments:
- cotangent: bfloat16 [32, 2048, 2048], P('dp', 'sp'), may hold values from -6 to 6
- unit_pre: bfloat16 [32, 2048, 2048], P('dp', None, 'sp'), may hold values from -6 to 6
- gate_pre: bfloat16 [32, 2048, 2048], P('dp', None, 'sp'), may hold values from -15 to 15
- out_weight: bfloat16 [2048, 2048], P('dp', 'sp'), may hold values from -0.125 to 0.125
- mix_weight: bfloat16 [8, 128, 128], replicated, may hold values from -0.5 to 0.5
- mix_bias: bfloat16 [8, 128], replicated, may hold values from 0.099609375 to 1.8984375
- norm_gain: bfloat16 [2048], P('sp'), may hold values from 0.099609375 to 1.8984375
- norm_shift: bfloat16 [2048], P('sp'), may hold values from -3 to 3
Outputs:
- unit_grad: bfloat16 [32, 2048, 2048], P('dp', None, 'sp')
- gate_grad: bfloat16 [32, 2048, 2048], P('dp', None, 'sp')
- out_weight_grad: float32 [2048, 2048], P('dp', 'sp')
- mix_weight_grad: float32 [8, 128, 128], replicated
- mix_bias_grad: float32 [8, 128], replicated
- gain_grad: float32 [2048], P('sp')
- shift_grad: float32 [2048], P('sp')
All inputs are finite; a program needn't handle non-finite values.
Results may differ from a plain program's by a relative error of at most 0.015.
Values may be sent and summed in bfloat16 or wider, within the bound.
A program may use at most 64 MiB of HBM per device.

v0:
```python
import math
import jax
import jax.numpy as jnp
from jax import lax
from jax.sharding import PartitionSpec as P

GW = 2048
GROUPS = 8
BLK = 128
epsilon = 1e-05
tanh_coef = math.sqrt(2.0 / math.pi)


def sum_over(x, axis):
    devices = lax.axis_size(axis)
    copies = jnp.broadcast_to(x[None], (devices, *x.shape))
    return lax.all_to_all(copies, axis, 0, 0, tiled=True).sum(axis=0)


def gelu_slope(values):
    inner = tanh_coef * (values + 0.044715 * values * values * values)
    hyper = jnp.tanh(inner)
    return 0.5 * (1.0 + hyper) + 0.5 * values * (1.0 - hyper * hyper) * tanh_coef * (
        1.0 + 3.0 * 0.044715 * values * values
    )


def local(cotangent, unit_pre, gate_pre, out_weight, mix_weight, mix_bias, norm_gain, norm_shift):
    seq_len = unit_pre.shape[1]
    channels = unit_pre.shape[2]
    group_dim = GW // GROUPS
    blocks = seq_len // BLK
    sp_size = lax.axis_size("sp")
    sp_at = lax.axis_index("sp")
    group = sp_at * channels // group_dim
    weight_rows = lax.all_gather(out_weight, "sp", axis=1, tiled=True)
    weight_whole = lax.all_gather(weight_rows, "dp", axis=0, tiled=True)
    units = unit_pre[0].astype(jnp.float32)
    gates = gate_pre[0].astype(jnp.float32)
    unit_act = jax.nn.gelu(units)
    gate_act = jax.nn.gelu(gates)
    moments = sum_over(
        jnp.stack([jnp.sum(gate_act, axis=-1), jnp.sum(gate_act * gate_act, axis=-1)]), "sp"
    )
    mean_val = moments[0] / GW
    var_val = moments[1] / GW - mean_val * mean_val
    rstd_val = lax.rsqrt(var_val + epsilon)
    centred = (gate_act - mean_val[:, None]) * rstd_val[:, None]
    gain_vec = norm_gain.astype(jnp.float32)
    normed = (centred * gain_vec + norm_shift.astype(jnp.float32)).astype(jnp.bfloat16)
    causal = jnp.arange(BLK)[:, None] >= jnp.arange(BLK)[None, :]
    local_weight = lax.dynamic_index_in_dim(mix_weight, group, 0, keepdims=False)
    masked = jnp.where(causal, local_weight, jnp.zeros_like(local_weight))
    local_bias = lax.dynamic_index_in_dim(mix_bias, group, 0, keepdims=False).astype(jnp.float32)
    normed_blocks = normed.reshape(blocks, BLK, channels)
    mixed = jnp.einsum("ts,nsd->ntd", masked, normed_blocks, preferred_element_type=jnp.float32)
    mixed = (mixed + local_bias[None, :, None]).reshape(seq_len, channels)
    gated = (unit_act * mixed).astype(jnp.bfloat16)
    gated_rows = lax.all_to_all(gated, "sp", split_axis=0, concat_axis=1, tiled=True)
    head_rows = jnp.dot(cotangent[0], weight_whole, preferred_element_type=jnp.float32)
    head = lax.all_to_all(
        head_rows.astype(jnp.bfloat16), "sp", split_axis=1, concat_axis=0, tiled=True
    ).astype(jnp.float32)
    weight_part = lax.dot_general(
        cotangent[0], gated_rows, (((0,), (0,)), ((), ())), preferred_element_type=jnp.float32
    ).astype(jnp.bfloat16)
    token_count = lax.axis_size("dp") * seq_len
    norm_scale = 1.0 / math.sqrt(token_count)
    mix_scale = 1.0 / math.sqrt(token_count // BLK * group_dim)
    plane_sum = lax.psum_scatter(weight_part, "dp", scatter_dimension=0, tiled=True)
    plane_parts = jnp.moveaxis(plane_sum.reshape(plane_sum.shape[0], sp_size, channels), 1, 0)
    arrived = lax.all_to_all(plane_parts, "sp", split_axis=0, concat_axis=0, tiled=True)
    out_grad = arrived.astype(jnp.float32).sum(axis=0) * norm_scale
    unit_grad = (head * mixed * gelu_slope(units)).astype(jnp.bfloat16)
    mix_grad = head * unit_act
    mix_round = mix_grad.astype(jnp.bfloat16).reshape(blocks, BLK, channels)
    mix_term = jnp.einsum(
        "ntd,nsd->ts", mix_round, normed_blocks, preferred_element_type=jnp.float32
    )
    mix_term = jnp.where(causal, mix_term, jnp.float32(0.0))
    bias_term = jnp.sum(mix_grad.reshape(blocks, BLK, channels), axis=(0, 2))
    normed_grad = jnp.einsum(
        "ts,ntd->nsd", masked, mix_round, preferred_element_type=jnp.float32
    ).reshape(seq_len, channels)
    gain_term = jnp.sum(normed_grad * centred, axis=0)
    shift_term = jnp.sum(normed_grad, axis=0)
    scaled = normed_grad * gain_vec
    back_sums = sum_over(
        jnp.stack([jnp.sum(scaled, axis=-1), jnp.sum(scaled * centred, axis=-1)]), "sp"
    )
    first_m = back_sums[0] / GW
    second_m = back_sums[1] / GW
    gate_grad = (
        rstd_val[:, None]
        * (scaled - first_m[:, None] - centred * second_m[:, None])
        * gelu_slope(gates)
    ).astype(jnp.bfloat16)
    group_hot = (jnp.arange(GROUPS) == group).astype(jnp.float32)
    own_hot = (jnp.arange(sp_size) == sp_at).astype(jnp.float32)
    packed = jnp.concatenate(
        [
            (group_hot[:, None, None] * mix_term).reshape(GROUPS * BLK, BLK),
            group_hot[:, None] * bias_term,
            own_hot[:, None] * gain_term,
            own_hot[:, None] * shift_term,
        ]
    )
    total = lax.psum(packed, ("sp", "dp"))
    top = GROUPS * BLK
    weight_total = total[:top].reshape(GROUPS, BLK, BLK)
    bias_total = total[top : top + GROUPS]
    tail = total[top + GROUPS :]
    gain_total = lax.dynamic_index_in_dim(tail, sp_at, 0, keepdims=False)
    shift_total = lax.dynamic_index_in_dim(tail, sp_size + sp_at, 0, keepdims=False)
    return (
        unit_grad[None],
        gate_grad[None],
        out_grad,
        weight_total * mix_scale,
        bias_total * mix_scale,
        gain_total * norm_scale,
        shift_total * norm_scale,
    )


def solution(mesh):
    return jax.shard_map(
        local,
        mesh=mesh,
        in_specs=(
            P("dp", "sp", None),
            P("dp", None, "sp"),
            P("dp", None, "sp"),
            P("dp", "sp"),
            P(),
            P(),
            P("sp"),
            P("sp"),
        ),
        out_specs=(
            P("dp", None, "sp"),
            P("dp", None, "sp"),
            P("dp", "sp"),
            P(),
            P(),
            P("sp"),
            P("sp"),
        ),
        check_vma=False,
    )
```

profile of v0, /device:TPU:32, one launch (start us, length us, event | category | flops | bytes accessed | tf_op | source)
XLA Modules:
  0.0 828.7 jit_solution(9951408123859522207)
XLA Ops:
  7.2 37.3 %all_gather.6 = bf16[64,2048]{1,0:T(8,128)(2,1)} all-gather(bf16[64,128]{1,0:T(8,128)(2,1)} %param.11), channel_id=1, replica_groups=mesh['sp'=16,'dp'=32] {'sp'}, dimensions={1}, use_global_device_ids=true | all-gather | bytes 278528 | tf_op jit(solution)/shard_map/all_gather | solution.py:36
  44.6 1.8 fusion.58
  47.2 8.9 %all-to-all-start.1 = ((f32[16,2,2048]{2,1,0:T(2,128)}), f32[16,2,2048]{2,1,0:T(2,128)S(1)}, u32[]{:S(2)}, u32[]{:S(2)}) async-start(f32[16,2,2048]{2,1,0:T(2,128)} %broadcast_in_dim.11), calls=%async_computation.1 | async-start | bytes 524288 | tf_op jit(solution)/shard_map/all_to_all | solution.py:17
  56.1 54.5 %all-gather.2.cloned.1.call-done = bf16[2048,2048]{1,0:T(8,128)(2,1)} async-done(((bf16[64,2048]{1,0:T(8,128)(2,1)}), bf16[2048,2048]{1,0:T(8,128)(2,1)}) %all-gather.2.cloned.1.call-update) | async-done | bytes 8388624 | tf_op jit(solution)/shard_map/all_gather | solution.py:37
  110.6 4.6 fusion.5
  116.2 12.7 %all-to-all-start = ((bf16[128,16,128]{2,0,1:T(8,128)(2,1)}), bf16[128,16,128]{2,0,1:T(8,128)(2,1)S(1)}, u32[]{:S(2)}, u32[]{:S(2)}) async-start(bf16[128,16,128]{2,0,1:T(8,128)(2,1)} %bitcast.135), calls=%async_computation | async-start | bytes 1048576 | tf_op jit(solution)/shard_map/all_to_all | solution.py:61
  129.0 29.5 %all-to-all-done = bf16[128,16,128]{2,0,1:T(8,128)(2,1)S(1)} async-done(((bf16[128,16,128]{2,0,1:T(8,128)(2,1)}), bf16[128,16,128]{2,0,1:T(8,128)(2,1)S(1)}, u32[]{:S(2)}, u32[]{:S(2)}) %all-to-all-start) | async-done | bytes 524320 | tf_op jit(solution)/shard_map/all_to_all | solution.py:61
  160.1 3.3 fusion.56
  164.2 6.1 all-to-all-start.2
  171.0 17.5 %all-to-all-done.2 = f32[16,2,2048]{2,1,0:T(2,128)S(1)} async-done(((f32[16,2,2048]{2,1,0:T(2,128)}), f32[16,2,2048]{2,1,0:T(2,128)S(1)}, u32[]{:S(2)}, u32[]{:S(2)}) %all-to-all-start.2) | async-done | bytes 262176 | tf_op jit(solution)/shard_map/all_to_all | solution.py:17
  188.7 2.8 fusion.51
  191.5 3.0 multiply_convert_fusion
  194.4 6.1 all-to-all-start.3
  200.9 2.5 fusion.6
  204.6 24.2 %all-to-all-done.3 = bf16[16,128,128]{2,1,0:T(8,128)(2,1)S(1)} async-done(((bf16[16,128,128]{2,1,0:T(8,128)(2,1)}), bf16[16,128,128]{2,1,0:T(8,128)(2,1)S(1)}, u32[]{:S(2)}, u32[]{:S(2)}) %all-to-all-start.3) | async-done | bytes 524320 | tf_op jit(solution)/shard_map/all_to_all | solution.py:59
  229.2 5.5 convert_bitcast_fusion
  234.7 12.4 %copy.42 = bf16[2048,2048]{1,0:T(8,128)(2,1)} copy(bf16[2048,2048]{0,1:T(8,128)(2,1)} %convert_bitcast_fusion) | data formatting | bytes 16777216
  247.1 423.4 %all-reduce.2.cloned.1.call-done = f32[1064,128]{1,0:T(8,128)} async-done(((f32[1064,128]{1,0:T(8,128)}), f32[1064,128]{1,0:T(8,128)}) %all-reduce.2.cloned.1.call-update) | async-done | bytes 544784 | tf_op jit(solution)/shard_map/psum | solution.py:108
  671.2 117.9 %reduce-scatter.4.cloned.1.call-done = bf16[64,2048]{1,0:T(8,128)(2,1)} async-done(((bf16[2048,2048]{1,0:T(8,128)(2,1)}), bf16[64,2048]{1,0:T(8,128)(2,1)}) %reduce-scatter.4.cloned.1.call-update) | async-done | bytes 262160
  791.3 12.7 %all-to-all-start.4 = ((bf16[16,64,128]{2,1,0:T(8,128)(2,1)}), bf16[16,64,128]{2,1,0:T(8,128)(2,1)S(1)}, u32[]{:S(2)}, u32[]{:S(2)}) async-start(bf16[16,64,128]{2,1,0:T(8,128)(2,1)} %bitcast.29), calls=%async_computation.4 | async-start | bytes 524288 | tf_op jit(solution)/shard_map/all_to_all | solution.py:72
  804.5 1.3 slice_multiply_fusion.5
  805.7 1.9 slice_multiply_fusion
  807.6 1.5 fusion.30
  809.1 12.2 %all-to-all-done.4 = bf16[16,64,128]{2,1,0:T(8,128)(2,1)S(1)} async-done(((bf16[16,64,128]{2,1,0:T(8,128)(2,1)}), bf16[16,64,128]{2,1,0:T(8,128)(2,1)S(1)}, u32[]{:S(2)}, u32[]{:S(2)}) %all-to-all-start.4) | async-done | bytes 262176 | tf_op jit(solution)/shard_map/all_to_all | solution.py:72
  (52 shorter events, 11.2 us)
Async XLA Ops:
  7.2 103.5 %copy-start = (bf16[1,128,2048]{2,1,0:T(8,128)(2,1)S(1)}, bf16[1,128,2048]{2,1,0:T(8,128)(2,1)}, u32[]{:S(2)}) copy-start(bf16[1,128,2048]{2,1,0:T(8,128)(2,1)} %param.8) | copy-start | bytes 1572868
  7.2 103.4 %all-gather.2.cloned.1.call-start = ((), (), s32[]{:S(2)}) async-start(), calls=%async_computation.6 | async-start | bytes 8650752 | tf_op jit(solution)/shard_map/all_gather | solution.py:37
  47.2 69.0 %all-to-all-start.1 = ((f32[16,2,2048]{2,1,0:T(2,128)}), f32[16,2,2048]{2,1,0:T(2,128)S(1)}, u32[]{:S(2)}, u32[]{:S(2)}) async-start(f32[16,2,2048]{2,1,0:T(2,128)} %broadcast_in_dim.11), calls=%async_computation.1 | async-start | bytes 524288 | tf_op jit(solution)/shard_map/all_to_all | solution.py:17
  56.1 72.8 %copy-start.5 = (bf16[128]{0:T(256)(128)(2,1)S(1)}, bf16[128]{0:T(256)(128)(2,1)}, u32[]{:S(2)}) copy-start(bf16[128]{0:T(256)(128)(2,1)} %param.14) | copy-start | bytes 772
  56.1 102.5 %copy-start.2 = (bf16[1,2048,128]{2,1,0:T(8,128)(2,1)S(1)}, bf16[1,2048,128]{2,1,0:T(8,128)(2,1)}, u32[]{:S(2)}) copy-start(bf16[1,2048,128]{2,1,0:T(8,128)(2,1)} %param.9) | copy-start | bytes 1572868
  56.1 104.0 %copy-start.1 = (bf16[1,2048,128]{2,1,0:T(8,128)(2,1)S(1)}, bf16[1,2048,128]{2,1,0:T(8,128)(2,1)}, u32[]{:S(2)}) copy-start(bf16[1,2048,128]{2,1,0:T(8,128)(2,1)} %param.10) | copy-start | bytes 1572868
  115.3 55.1 %copy-start.6 = (bf16[128]{0:T(256)(128)(2,1)S(1)}, bf16[128]{0:T(256)(128)(2,1)}, u32[]{:S(2)}) copy-start(bf16[128]{0:T(256)(128)(2,1)} %param.15) | copy-start | bytes 772
  116.2 42.4 %all-to-all-start = ((bf16[128,16,128]{2,0,1:T(8,128)(2,1)}), bf16[128,16,128]{2,0,1:T(8,128)(2,1)S(1)}, u32[]{:S(2)}, u32[]{:S(2)}) async-start(bf16[128,16,128]{2,0,1:T(8,128)(2,1)} %bitcast.135), calls=%async_computation | async-start | bytes 1048576 | tf_op jit(solution)/shard_map/all_to_all | solution.py:61
  159.1 1.0 copy-start.3
  164.2 24.4 %all-to-all-start.2 = ((f32[16,2,2048]{2,1,0:T(2,128)}), f32[16,2,2048]{2,1,0:T(2,128)S(1)}, u32[]{:S(2)}, u32[]{:S(2)}) async-start(f32[16,2,2048]{2,1,0:T(2,128)} %broadcast_in_dim.15), calls=%async_computation.2 | async-start | bytes 524288 | tf_op jit(solution)/shard_map/all_to_all | solution.py:17
  194.4 34.5 %all-to-all-start.3 = ((bf16[16,128,128]{2,1,0:T(8,128)(2,1)}), bf16[16,128,128]{2,1,0:T(8,128)(2,1)S(1)}, u32[]{:S(2)}, u32[]{:S(2)}) async-start(bf16[16,128,128]{2,1,0:T(8,128)(2,1)} %get-tuple-element.36), calls=%async_computation.3 | async-start | bytes 1048576 | tf_op jit(solution)/shard_map/all_to_all | solution.py:59
  200.5 470.0 %all-reduce.2.cloned.1.call-start = ((), (), s32[]{:S(2)}) async-start(), calls=%async_computation.7 | async-start | bytes 1089536 | tf_op jit(solution)/shard_map/psum | solution.py:108
  204.6 584.5 %reduce-scatter.4.cloned.1.call-start = ((), (), s32[]{:S(2)}) async-start(), calls=%async_computation.8 | async-start | bytes 8650752
  247.1 560.5 %copy-start.4 = (f32[16,128,128]{2,1,0:T(8,128)S(1)}, f32[16,128,128]{2,1,0:T(8,128)}, u32[]{:S(2)}) copy-start(f32[16,128,128]{2,1,0:T(8,128)} %get-tuple-element.37) | copy-start | bytes 3145732
  791.3 30.0 %all-to-all-start.4 = ((bf16[16,64,128]{2,1,0:T(8,128)(2,1)}), bf16[16,64,128]{2,1,0:T(8,128)(2,1)S(1)}, u32[]{:S(2)}, u32[]{:S(2)}) async-start(bf16[16,64,128]{2,1,0:T(8,128)(2,1)} %bitcast.29), calls=%async_computation.4 | async-start | bytes 524288 | tf_op jit(solution)/shard_map/all_to_all | solution.py:72
Sparse Core Ops, SparseCore 0:
  44.7 65.8 all-gather.1
  206.8 463.6 all-reduce.1
  675.1 114.0 reduce-scatter.3
where the time goes:
time: 830 us; the launch traced here: 829 us
  waiting for transfers between devices  679 us (82%)
  starting transfers between devices  46.6 us (6%)
  blocking collectives  37.3 us (4%)
  local copies, waits for them, and re-layouts  19.8 us (2%)
  matrix products  18.9 us (2%)
  between operations  13.9 us (2%)
  other arithmetic  12.7 us (2%)
    psum x1, waiting for transfers between devices, local(): total = lax.psum(packed, ('sp', 'dp'))  423 us
    unnamed x4, waiting for transfers between devices  118 us
    all_gather x1, waiting for transfers between devices, local(): weight_whole = lax.all_gather(weight_rows, 'dp', axis=0, tiled=True)  54.5 us
    all_gather x1, blocking collectives, local(): weight_rows = lax.all_gather(out_weight, 'sp', axis=1, tiled=True)  37.3 us
    all_to_all x1, waiting for transfers between devices, local(): lax.all_to_all(head_rows.astype(jnp.bfloat16), 'sp', split_axis=1, concat...  29.5 us
    all_to_all x1, waiting for transfers between devices, local(): lax.all_to_all(gated, 'sp', split_axis=0, concat_axis=1, tiled=True)  24.2 us
    all_to_all x2, waiting for transfers between devices, sum_over(): return lax.all_to_all(copies, axis, 0, 0, tiled=True).sum(axis=0)  17.5 us
  transfers between devices with their start and end apart: 8, of which 7 were waited for; matrix products, arithmetic and copies ran while one was open for 4% of the time, Pallas kernels for 0%

commit v1 on v0

--- a/solution.py
+++ b/solution.py
@@ -9,6 +9,12 @@
 BLK = 128
 epsilon = 1e-05
 tanh_coef = math.sqrt(2.0 / math.pi)
+
+
+def _find_cells(array_in, dev_axis, link_axis):
+    for j in (dev_axis, link_axis):
+        array_in = lax.psum(array_in, j)
+    return array_in
 
 
 def sum_over(x, axis):
@@ -105,7 +111,7 @@
             own_hot[:, None] * shift_term,
         ]
     )
-    total = lax.psum(packed, ("sp", "dp"))
+    total = _find_cells(packed, "dp", "sp")
     top = GROUPS * BLK
     weight_total = total[:top].reshape(GROUPS, BLK, BLK)
     bias_total = total[top : top + GROUPS]

time: 830 us -> 635 us (0.77)
  waiting for transfers between devices: 679 us -> 484 us
    psum x1 -> x2, waiting for transfers between devices: 423 us -> 254 us  [_find_cells(): array_in = lax.psum(array_in, j)]
    all_to_all x1, waiting for transfers between devices: 24.2 us -> 0.01 us  [local(): lax.all_to_all(gated, 'sp', split_axis=0, concat_axis=1, tiled=True)]
    unnamed x4 -> x5, waiting for transfers between devices: 118 us -> 116 us
  transfers between devices with their start and end apart: 8 -> 9, of which waited for: 7 -> 7; matrix products, arithmetic and copies ran while one was open for 4% -> 6% of each run, Pallas kernels for 0% -> 0%
where the time goes in v1:
time: 635 us; the launch traced here: 633 us
  waiting for transfers between devices  484 us (76%)
  starting transfers between devices  46.6 us (7%)
  blocking collectives  37.3 us (6%)
  local copies, waits for them, and re-layouts  19.8 us (3%)
  matrix products  19 us (3%)
  between operations  13.9 us (2%)
  other arithmetic  12.7 us (2%)
    psum x2, waiting for transfers between devices, _find_cells(): array_in = lax.psum(array_in, j)  254 us
    unnamed x5, waiting for transfers between devices  116 us
    all_gather x1, waiting for transfers between devices, local(): weight_whole = lax.all_gather(weight_rows, 'dp', axis=0, tiled=True)  54.5 us
    all_gather x1, blocking collectives, local(): weight_rows = lax.all_gather(out_weight, 'sp', axis=1, tiled=True)  37.3 us
    all_to_all x1, waiting for transfers between devices, local(): lax.all_to_all(head_rows.astype(jnp.bfloat16), 'sp', split_axis=1, concat...  29.5 us
    all_to_all x2, waiting for transfers between devices, sum_over(): return lax.all_to_all(copies, axis, 0, 0, tiled=True).sum(axis=0)  17.5 us
    unnamed x18, local copies, waits for them, and re-layouts  15.4 us
    all_to_all x2, starting transfers between devices, sum_over(): return lax.all_to_all(copies, axis, 0, 0, tiled=True).sum(axis=0)  15 us
  transfers between devices with their start and end apart: 9, of which 7 were waited for; matrix products, arithmetic and copies ran while one was open for 6% of the time, Pallas kernels for 0%

profile of v1, /device:TPU:32, one launch (start us, length us, event | category | flops | bytes accessed | tf_op | source)
XLA Modules:
  0.0 633.3 jit_solution(16026258284083626327)
XLA Ops:
  7.2 37.3 %all_gather.6 = bf16[64,2048]{1,0:T(8,128)(2,1)} all-gather(bf16[64,128]{1,0:T(8,128)(2,1)} %param.11), channel_id=1, replica_groups=mesh['sp'=16,'dp'=32] {'sp'}, dimensions={1}, use_global_device_ids=true | all-gather | bytes 278528 | tf_op jit(solution)/shard_map/all_gather | solution.py:42
  44.6 1.8 fusion.58
  47.2 8.9 %all-to-all-start.1 = ((f32[16,2,2048]{2,1,0:T(2,128)}), f32[16,2,2048]{2,1,0:T(2,128)S(1)}, u32[]{:S(2)}, u32[]{:S(2)}) async-start(f32[16,2,2048]{2,1,0:T(2,128)} %broadcast_in_dim.11), calls=%async_computation.1 | async-start | bytes 524288 | tf_op jit(solution)/shard_map/all_to_all | solution.py:23
  56.1 54.5 %all-gather.2.cloned.1.call-done = bf16[2048,2048]{1,0:T(8,128)(2,1)} async-done(((bf16[64,2048]{1,0:T(8,128)(2,1)}), bf16[2048,2048]{1,0:T(8,128)(2,1)}) %all-gather.2.cloned.1.call-update) | async-done | bytes 8388624 | tf_op jit(solution)/shard_map/all_gather | solution.py:43
  110.6 4.6 fusion.5
  116.2 12.7 %all-to-all-start = ((bf16[128,16,128]{2,0,1:T(8,128)(2,1)}), bf16[128,16,128]{2,0,1:T(8,128)(2,1)S(1)}, u32[]{:S(2)}, u32[]{:S(2)}) async-start(bf16[128,16,128]{2,0,1:T(8,128)(2,1)} %bitcast.135), calls=%async_computation | async-start | bytes 1048576 | tf_op jit(solution)/shard_map/all_to_all | solution.py:67
  129.0 29.5 %all-to-all-done = bf16[128,16,128]{2,0,1:T(8,128)(2,1)S(1)} async-done(((bf16[128,16,128]{2,0,1:T(8,128)(2,1)}), bf16[128,16,128]{2,0,1:T(8,128)(2,1)S(1)}, u32[]{:S(2)}, u32[]{:S(2)}) %all-to-all-start) | async-done | bytes 524320 | tf_op jit(solution)/shard_map/all_to_all | solution.py:67
  160.1 3.3 fusion.56
  164.2 6.1 all-to-all-start.2
  171.0 17.5 %all-to-all-done.2 = f32[16,2,2048]{2,1,0:T(2,128)S(1)} async-done(((f32[16,2,2048]{2,1,0:T(2,128)}), f32[16,2,2048]{2,1,0:T(2,128)S(1)}, u32[]{:S(2)}, u32[]{:S(2)}) %all-to-all-start.2) | async-done | bytes 262176 | tf_op jit(solution)/shard_map/all_to_all | solution.py:23
  188.7 2.8 fusion.51
  191.5 3.0 multiply_convert_fusion
  194.4 6.1 all-to-all-start.3
  200.9 2.5 fusion.6
  204.7 132.2 %all-reduce.3.cloned.1.call-done = f32[1064,128]{1,0:T(8,128)} async-done(((f32[1064,128]{1,0:T(8,128)}), f32[1064,128]{1,0:T(8,128)}) %all-reduce.3.cloned.1.call-update) | async-done | bytes 544784 | tf_op jit(solution)/shard_map/psum | solution.py:16
  337.3 5.5 convert_bitcast_fusion
  342.8 12.3 %copy.42 = bf16[2048,2048]{1,0:T(8,128)(2,1)} copy(bf16[2048,2048]{0,1:T(8,128)(2,1)} %convert_bitcast_fusion) | data formatting | bytes 16777216
  355.2 121.6 %all-reduce.5.cloned.1.call-done = f32[1064,128]{1,0:T(8,128)} async-done(((f32[1064,128]{1,0:T(8,128)}), f32[1064,128]{1,0:T(8,128)}) %all-reduce.5.cloned.1.call-update) | async-done | bytes 544784 | tf_op jit(solution)/shard_map/psum | solution.py:16
  477.5 116.3 %reduce-scatter.4.cloned.1.call-done = bf16[64,2048]{1,0:T(8,128)(2,1)} async-done(((bf16[2048,2048]{1,0:T(8,128)(2,1)}), bf16[64,2048]{1,0:T(8,128)(2,1)}) %reduce-scatter.4.cloned.1.call-update) | async-done | bytes 262160
  595.9 12.7 %all-to-all-start.4 = ((bf16[16,64,128]{2,1,0:T(8,128)(2,1)}), bf16[16,64,128]{2,1,0:T(8,128)(2,1)S(1)}, u32[]{:S(2)}, u32[]{:S(2)}) async-start(bf16[16,64,128]{2,1,0:T(8,128)(2,1)} %bitcast.29), calls=%async_computation.4 | async-start | bytes 524288 | tf_op jit(solution)/shard_map/all_to_all | solution.py:78
  609.0 1.3 slice_multiply_fusion.5
  610.3 1.9 slice_multiply_fusion
  612.2 1.5 fusion.30
  613.7 12.2 %all-to-all-done.4 = bf16[16,64,128]{2,1,0:T(8,128)(2,1)S(1)} async-done(((bf16[16,64,128]{2,1,0:T(8,128)(2,1)}), bf16[16,64,128]{2,1,0:T(8,128)(2,1)S(1)}, u32[]{:S(2)}, u32[]{:S(2)}) %all-to-all-start.4) | async-done | bytes 262176 | tf_op jit(solution)/shard_map/all_to_all | solution.py:78
  (55 shorter events, 11.2 us)
Async XLA Ops:
  7.2 103.5 %copy-start = (bf16[1,128,2048]{2,1,0:T(8,128)(2,1)S(1)}, bf16[1,128,2048]{2,1,0:T(8,128)(2,1)}, u32[]{:S(2)}) copy-start(bf16[1,128,2048]{2,1,0:T(8,128)(2,1)} %param.8) | copy-start | bytes 1572868
  7.2 103.4 %all-gather.2.cloned.1.call-start = ((), (), s32[]{:S(2)}) async-start(), calls=%async_computation.6 | async-start | bytes 8650752 | tf_op jit(solution)/shard_map/all_gather | solution.py:43
  47.2 69.0 %all-to-all-start.1 = ((f32[16,2,2048]{2,1,0:T(2,128)}), f32[16,2,2048]{2,1,0:T(2,128)S(1)}, u32[]{:S(2)}, u32[]{:S(2)}) async-start(f32[16,2,2048]{2,1,0:T(2,128)} %broadcast_in_dim.11), calls=%async_computation.1 | async-start | bytes 524288 | tf_op jit(solution)/shard_map/all_to_all | solution.py:23
  56.1 72.8 %copy-start.5 = (bf16[128]{0:T(256)(128)(2,1)S(1)}, bf16[128]{0:T(256)(128)(2,1)}, u32[]{:S(2)}) copy-start(bf16[128]{0:T(256)(128)(2,1)} %param.14) | copy-start | bytes 772
  56.1 102.5 %copy-start.2 = (bf16[1,2048,128]{2,1,0:T(8,128)(2,1)S(1)}, bf16[1,2048,128]{2,1,0:T(8,128)(2,1)}, u32[]{:S(2)}) copy-start(bf16[1,2048,128]{2,1,0:T(8,128)(2,1)} %param.9) | copy-start | bytes 1572868
  56.1 104.0 %copy-start.1 = (bf16[1,2048,128]{2,1,0:T(8,128)(2,1)S(1)}, bf16[1,2048,128]{2,1,0:T(8,128)(2,1)}, u32[]{:S(2)}) copy-start(bf16[1,2048,128]{2,1,0:T(8,128)(2,1)} %param.10) | copy-start | bytes 1572868
  115.3 55.1 %copy-start.6 = (bf16[128]{0:T(256)(128)(2,1)S(1)}, bf16[128]{0:T(256)(128)(2,1)}, u32[]{:S(2)}) copy-start(bf16[128]{0:T(256)(128)(2,1)} %param.15) | copy-start | bytes 772
  116.2 42.4 %all-to-all-start = ((bf16[128,16,128]{2,0,1:T(8,128)(2,1)}), bf16[128,16,128]{2,0,1:T(8,128)(2,1)S(1)}, u32[]{:S(2)}, u32[]{:S(2)}) async-start(bf16[128,16,128]{2,0,1:T(8,128)(2,1)} %bitcast.135), calls=%async_computation | async-start | bytes 1048576 | tf_op jit(solution)/shard_map/all_to_all | solution.py:67
  159.1 1.0 copy-start.3
  164.2 24.4 %all-to-all-start.2 = ((f32[16,2,2048]{2,1,0:T(2,128)}), f32[16,2,2048]{2,1,0:T(2,128)S(1)}, u32[]{:S(2)}, u32[]{:S(2)}) async-start(f32[16,2,2048]{2,1,0:T(2,128)} %broadcast_in_dim.15), calls=%async_computation.2 | async-start | bytes 524288 | tf_op jit(solution)/shard_map/all_to_all | solution.py:23
  194.4 142.6 %all-to-all-start.3 = ((bf16[16,128,128]{2,1,0:T(8,128)(2,1)}), bf16[16,128,128]{2,1,0:T(8,128)(2,1)S(1)}, u32[]{:S(2)}, u32[]{:S(2)}) async-start(bf16[16,128,128]{2,1,0:T(8,128)(2,1)} %get-tuple-element.36), calls=%async_computation.3 | async-start | bytes 1048576 | tf_op jit(solution)/shard_map/all_to_all | solution.py:65
  200.5 136.4 %all-reduce.3.cloned.1.call-start = ((), (), s32[]{:S(2)}) async-start(), calls=%async_computation.7 | async-start | bytes 1089536 | tf_op jit(solution)/shard_map/psum | solution.py:16
  204.6 272.2 %all-reduce.5.cloned.1.call-start = ((), (), s32[]{:S(2)}) async-start(), calls=%async_computation.8 | async-start | bytes 1089536 | tf_op jit(solution)/shard_map/psum | solution.py:16
  336.9 256.8 %reduce-scatter.4.cloned.1.call-start = ((), (), s32[]{:S(2)}) async-start(), calls=%async_computation.9 | async-start | bytes 8650752
  355.2 257.0 %copy-start.4 = (f32[16,128,128]{2,1,0:T(8,128)S(1)}, f32[16,128,128]{2,1,0:T(8,128)}, u32[]{:S(2)}) copy-start(f32[16,128,128]{2,1,0:T(8,128)} %get-tuple-element.37) | copy-start | bytes 3145732
  595.9 30.0 %all-to-all-start.4 = ((bf16[16,64,128]{2,1,0:T(8,128)(2,1)}), bf16[16,64,128]{2,1,0:T(8,128)(2,1)S(1)}, u32[]{:S(2)}, u32[]{:S(2)}) async-start(bf16[16,64,128]{2,1,0:T(8,128)(2,1)} %bitcast.29), calls=%async_computation.4 | async-start | bytes 524288 | tf_op jit(solution)/shard_map/all_to_all | solution.py:78
Sparse Core Ops, SparseCore 0:
  44.7 65.8 all-gather.1
  204.7 132.1 all-reduce.2
  339.2 137.4 all-reduce.4
  481.2 112.4 reduce-scatter.3
